TPU v7x, 32 devices: a whole 2x2x4 slice. The times are simulated.
32 devices in a mesh: ep: 8 (over z, core), tp: 4 (over y, x).
Axes of the slice: x: 2, y: 2, z: 4, core: 2. Of those that a mesh axis runs over, the one named last changes fastest.
Arguments:
- pool_input: bfloat16 [2048, 2048], P('ep'), may hold values from -6 to 6
- pool_gain: float32 [2048], replicated, may hold values from 0.1 to 1.9
- pool_weight: bfloat16 [512, 2048], P(None, 'tp'), may hold values from -0.25 to 0.25
- pool_scale: float32 [2048], P('tp'), may hold values from 0.1 to 1.9
- moe_input: bfloat16 [1536, 2048], P('ep'), may hold values from -6 to 6
- moe_gain: float32 [2048], replicated, may hold values from 0.1 to 1.9
- routes: int32 [1536, 2], P('ep'), may hold values from 0 to 7, all different within a row; in each aligned block of 192 rows (0 to 191, 192 to 383, ...) at most 96 rows name the same one
- route_logits: float32 [1536, 2], P('ep'), may hold values from -4 to 4
- gate_weight: bfloat16 [8, 2048, 4096], P('ep', None, 'tp'), may hold values from -0.125 to 0.125
- up_weight: bfloat16 [8, 2048, 4096], P('ep', None, 'tp'), may hold values from -0.125 to 0.125
- down_weight: bfloat16 [8, 2048, 4096], P('ep', None, 'tp'), may hold values from -0.09375 to 0.09375
Outputs:
- pool_out: bfloat16 [2048, 2048], P('ep', 'tp')
- expert_out: bfloat16 [1536, 2048], P('ep', 'tp')
Inputs may be any that keep to these rules, and one draw needn't show every extreme that they name: `routes`: the 2 experts of a token differ. Within the rows of one device (aligned blocks of 192 rows) no expert is named by more than 96 rows, and in every draw some expert is named by exactly 96 rows of some device.
All inputs are finite; a program needn't handle non-finite values.
Results may differ from a plain program's by a relative error of at most 0.017.
Values may be sent and summed in bfloat16 or wider, within the bound.
A program may use at most 64 MiB of HBM per device.

v0:
```python
import jax
import jax.numpy as jnp
from jax import lax
from jax.sharding import PartitionSpec as P

GROUP_WIDTH = 512
EPSILON = 1e-06
halo_rows = 15


def passed_along(value, axis, steps):
    count = lax.axis_size(axis)
    leading, last = (max(0, -steps), min(count, count - steps))
    return lax.ppermute(value, axis, [(source, source + steps) for source in range(leading, last)])


def rms_rows(row_block, scale_gain):
    values = row_block.astype(jnp.float32)
    scaled = values * lax.rsqrt(jnp.mean(values * values, axis=-1, keepdims=True) + EPSILON)
    return (scaled * scale_gain).astype(jnp.bfloat16)


def delayed(values, offset):
    return jnp.concatenate(
        [jnp.zeros((offset,) + values.shape[1:], values.dtype), values[:-offset]], axis=0
    )


def window_sums(values):
    totals = []
    current = values
    for offset in (1, 2, 4, 8):
        current = current + delayed(current, offset)
        totals.append(current)
    return totals


def slot_tables(route_block, expert_count, capacity):
    tokens_count = route_block.shape[0]
    picks_count = route_block.shape[1]
    flat_ids = route_block.reshape(-1)
    onehot = (flat_ids[:, None] == jnp.arange(expert_count, dtype=jnp.int32)[None, :]).astype(
        jnp.int32
    )
    before = jnp.cumsum(onehot, axis=0) - onehot
    rank_in = jnp.sum(before * onehot, axis=1)
    slot_ids = flat_ids * capacity + rank_in
    owners = jnp.repeat(jnp.arange(tokens_count, dtype=jnp.int32), picks_count)
    holder = jnp.full((expert_count * capacity,), tokens_count, jnp.int32).at[slot_ids].set(owners)
    return (slot_ids, holder)


def pool_half(pool_input, pool_gain, pool_weight, pool_scale):
    normed = rms_rows(pool_input, pool_gain)
    local_rows = normed.shape[0]
    column_count = pool_weight.shape[1]
    group_index = lax.axis_index("tp") * column_count // GROUP_WIDTH
    own_group = lax.dynamic_slice_in_dim(normed, group_index * GROUP_WIDTH, GROUP_WIDTH, 1)
    earlier = passed_along(own_group[local_rows - halo_rows :], "ep", 1)
    extended = jnp.concatenate([earlier, own_group], axis=0).astype(jnp.float32)
    stacked = jnp.stack(window_sums(extended))[:, halo_rows:]
    chosen = lax.dynamic_index_in_dim(stacked, group_index, 0, keepdims=False)
    position = lax.axis_index("ep") * local_rows + lax.iota(jnp.int32, local_rows)
    window = jnp.left_shift(jnp.int32(2), group_index)
    counts = jnp.minimum(position + 1, window).astype(jnp.float32)
    mixed_in = (chosen / counts[:, None] - own_group.astype(jnp.float32)).astype(jnp.bfloat16)
    product = jnp.dot(mixed_in, pool_weight, preferred_element_type=jnp.float32)
    return (product * pool_scale).astype(jnp.bfloat16)


def expert_half(moe_input, moe_gain, routes, route_logits, gate_weight, up_weight, down_weight):
    normed = rms_rows(moe_input, moe_gain)
    local_rows, row_width = normed.shape
    picks_count = routes.shape[1]
    experts = lax.axis_size("ep")
    capacity = 2 * local_rows * picks_count // experts
    slot_ids, holder = slot_tables(routes, experts, capacity)
    padded = jnp.concatenate([normed, jnp.zeros((1, row_width), jnp.bfloat16)], axis=0)
    gate_block = gate_weight[0]
    up_block = up_weight[0]
    down_block = down_weight[0]
    column_count = row_width // lax.axis_size("tp")
    start_col = lax.axis_index("tp") * column_count
    narrow = lax.dynamic_slice_in_dim(padded, start_col, column_count, 1)
    outgoing = narrow[holder].reshape(experts, capacity, column_count)
    arrived = lax.all_to_all(outgoing, "ep", split_axis=0, concat_axis=0, tiled=True).reshape(
        experts * capacity, column_count
    )
    segment = lax.all_gather(arrived, "tp", axis=1, tiled=True)
    gate_part = jnp.dot(segment, gate_block, preferred_element_type=jnp.float32)
    up_part = jnp.dot(segment, up_block, preferred_element_type=jnp.float32)
    hidden = (jax.nn.silu(gate_part) * up_part).astype(jnp.bfloat16)
    summed = lax.psum_scatter(
        lax.dot_general(
            down_block, hidden, (((1,), (1,)), ((), ())), preferred_element_type=jnp.float32
        ).astype(jnp.bfloat16),
        "tp",
        scatter_dimension=0,
        tiled=True,
    ).astype(jnp.float32)
    results = summed.astype(jnp.bfloat16).reshape(summed.shape[0], experts, capacity)
    returned = lax.all_to_all(results, "ep", split_axis=1, concat_axis=1, tiled=True).reshape(
        summed.shape[0], experts * capacity
    )
    picked = (
        returned[:, slot_ids].astype(jnp.float32).reshape(summed.shape[0], local_rows, picks_count)
    )
    raised = jnp.exp(route_logits)
    shares = raised / jnp.sum(raised, axis=-1, keepdims=True)
    combined = jnp.einsum("dtk,tk->td", picked, shares)
    return combined.astype(jnp.bfloat16)


def local(
    pool_input,
    pool_gain,
    pool_weight,
    pool_scale,
    moe_input,
    moe_gain,
    routes,
    route_logits,
    gate_weight,
    up_weight,
    down_weight,
):
    pool_out = pool_half(pool_input, pool_gain, pool_weight, pool_scale)
    expert_out = expert_half(
        moe_input, moe_gain, routes, route_logits, gate_weight, up_weight, down_weight
    )
    return (pool_out, expert_out)


def solution(mesh):
    in_specs = (
        P("ep", None),
        P(),
        P(None, "tp"),
        P("tp"),
        P("ep", None),
        P(),
        P("ep", None),
        P("ep", None),
        P("ep", None, "tp"),
        P("ep", None, "tp"),
        P("ep", None, "tp"),
    )
    out_specs = (P("ep", "tp"), P("ep", "tp"))
    return jax.shard_map(local, mesh=mesh, in_specs=in_specs, out_specs=out_specs, check_vma=False)
```

profile of v0, /device:TPU:0, one launch (start us, length us, event | category | flops | bytes accessed | tf_op | source)
XLA Modules:
  0.0 184.2 jit_solution(8326187543108541298)
XLA Ops:
  7.2 0.0 copy-start
  7.2 0.0 all-gather.2.cloned.1.call-start
  7.2 0.8 copy.14
  8.1 0.1 eq.29
  8.2 0.1 eq.25
  8.4 0.7 broadcast_multiply_fusion
  9.1 1.4 fusion.14
  10.4 0.9 reduce-window.6
  11.3 0.2 slice_reduce_fusion
  11.6 0.1 copy.13
  11.7 0.1 mul.99
  11.9 0.1 reshape.122
  12.0 0.1 fusion.29
  12.1 2.9 %scatter_custom_fusion = s32[768]{0:T(1024)S(1)} fusion(s32[384]{0:T(512)S(1)} %fusion.33, s32[384]{0:T(512)S(1)} %reshape.122, s32[]{:T(128)} %constant.67.clone.1), kind=kCustom, calls=%fused_computation.53 | custom fusion | bytes 3076 | tf_op jit(solution)/shard_map/scatter | solution.py:49
  15.1 1.4 fusion.16
  16.5 2.7 %gather_fusion = bf16[768,512]{1,0:T(8,128)(2,1)S(1)} fusion(bf16[193,512]{1,0:T(8,128)(2,1)S(1)} %pad_dynamic-slice_fusion.4, s32[1024]{0:T(1024)S(1)} %pad_clamp_fusion.1), kind=kCustom, calls=%fused_computation | custom fusion | bytes 1575936 | tf_op jit(solution)/shard_map/gather | solution.py:85
  19.2 27.2 %all_to_all.10 = bf16[8,96,512]{2,1,0:T(8,128)(2,1)} all-to-all(bf16[8,96,512]{2,1,0:T(8,128)(2,1)S(1)} %bitcast.67), channel_id=1, replica_groups=mesh['ep'=8,'tp'=4] {'ep'}, dimensions={0} | all-to-all | bytes 1572864 | tf_op jit(solution)/shard_map/all_to_all | solution.py:86
  46.4 0.0 all-gather.2.cloned.1.call-update
  46.4 0.0 reduce-scatter.2.cloned.1.call-start
  46.5 42.8 %all-gather.2.cloned.1.call-done = bf16[768,2048]{1,0:T(8,128)(2,1)} async-done(((bf16[768,512]{1,0:T(8,128)(2,1)}), bf16[768,2048]{1,0:T(8,128)(2,1)}) %all-gather.2.cloned.1.call-update) | async-done | bytes 3145744 | tf_op jit(solution)/shard_map/all_gather | solution.py:89
  89.2 0.0 copy-start.3
  89.2 0.0 copy-start.5
  89.2 6.3 %fusion.2 = f32[768,1024]{1,0:T(8,128)S(1)} fusion(bf16[768,2048]{1,0:T(8,128)(2,1)} %all-gather.2.cloned.1.call-done, bf16[1,2048,1024]{2,1,0:T(8,128)(2,1)} %param.20), kind=kOutput, calls=%fused_computation.5 | convolution fusion | flops 3221225472 | bytes 10485760 | tf_op jit(solution)/shard_map/dot_general | solution.py:91
  95.5 0.0 copy-done.3
  95.5 0.0 copy-done.5
  95.5 0.0 copy-start.4
  95.5 3.8 %multiply_convert_fusion = bf16[768,1024]{1,0:T(8,128)(2,1)S(1)} fusion(f32[768,1024]{1,0:T(8,128)S(1)} %fusion.2, bf16[768,2048]{1,0:T(8,128)(2,1)S(1)} %copy-done.5, bf16[1,2048,1024]{2,1,0:T(8,128)(2,1)S(1)} %copy-done.3), kind=kOutput, calls=%fused_computation.10 | convolution fusion | flops 3225944064 | bytes 12058624 | tf_op jit(solution)/shard_map/dot_general | solution.py:90
  99.4 0.0 copy-done.4
  99.4 4.9 %fusion.9 = bf16[2048,768]{0,1:T(8,128)(2,1)} fusion(bf16[768,1024]{1,0:T(8,128)(2,1)S(1)} %multiply_convert_fusion, bf16[1,2048,1024]{2,1,0:T(8,128)(2,1)S(1)} %copy-done.4), kind=kOutput, calls=%fused_computation.11 | convolution fusion | flops 3222798336 | bytes 8912896 | tf_op jit(solution)/shard_map/dot_general | solution.py:94
  104.3 0.0 copy-start.1
  104.3 0.0 reduce-scatter.2.cloned.1.call-update
  104.3 0.0 copy-start.2
  104.3 1.2 copy-done.1
  105.5 1.6 convert_element_type.53
  107.1 0.8 dynamic-slice
  107.9 0.3 multiply_reduce_fusion
  108.1 1.2 fusion.25
  109.3 1.6 collective-permute-start
  110.9 0.0 copy-done.2
  111.0 37.4 %reduce-scatter.2.cloned.1.call-done = bf16[512,768]{0,1:T(8,128)(2,1)} async-done(((bf16[2048,768]{0,1:T(8,128)(2,1)}), bf16[512,768]{0,1:T(8,128)(2,1)}) %reduce-scatter.2.cloned.1.call-update) | async-done | bytes 786448 | tf_op jit(solution)/shard_map/reduce_scatter | solution.py:93
  148.3 4.6 %all-to-all-start.1 = ((bf16[512,8,96]{0,2,1:T(8,128)(2,1)}), bf16[512,8,96]{0,2,1:T(8,128)(2,1)S(1)}, u32[]{:S(2)}, u32[]{:S(2)}) async-start(bf16[512,8,96]{0,2,1:T(8,128)(2,1)} %bitcast.71), calls=%async_computation.2 | async-start | bytes 1572864 | tf_op jit(solution)/shard_map/all_to_all | solution.py:102
  153.0 0.2 copy.16
  153.2 0.0 collective-permute-done
  153.2 0.1 maximum_convert_fusion
  153.3 0.1 pad_add_fusion.2
  153.4 0.0 copy-start.6
  153.4 0.1 pad_add_fusion.1
  153.5 0.1 pad_add_fusion
  153.7 0.1 add_bitcast_fusion
  153.8 0.0 copy-done
  153.8 0.3 copy-done.6
  154.1 1.2 fusion.17
  155.3 18.6 %all-to-all-done.1 = bf16[512,8,96]{0,2,1:T(8,128)(2,1)S(1)} async-done(((bf16[512,8,96]{0,2,1:T(8,128)(2,1)}), bf16[512,8,96]{0,2,1:T(8,128)(2,1)S(1)}, u32[]{:S(2)}, u32[]{:S(2)}) %all-to-all-start.1) | async-done | bytes 786464 | tf_op jit(solution)/shard_map/all_to_all | solution.py:102
  173.9 2.1 %gather_fusion.1 = bf16[384,512]{1,0:T(8,128)(2,1)S(1)} fusion(bf16[512,768]{0,1:T(8,128)(2,1)S(1)} %bitcast.61, s32[1024]{0:T(1024)S(1)} %pad_clamp_fusion), kind=kCustom, calls=%fused_computation.1 | custom fusion | bytes 787968 | tf_op jit(solution)/shard_map/gather | solution.py:106
  176.0 0.2 reshape.101
  176.1 0.6 fusion.36
  176.7 0.7 copy.19
  (15 shorter events, 0.2 us)
Async XLA Ops:
  7.2 146.6 %copy-start = (bf16[512,512]{1,0:T(8,128)(2,1)S(1)}, bf16[512,512]{1,0:T(8,128)(2,1)}, u32[]{:S(2)}) copy-start(bf16[512,512]{1,0:T(8,128)(2,1)} %param.13) | copy-start | bytes 1572868
  7.2 82.0 %all-gather.2.cloned.1.call-start = ((), (), s32[]{:S(2)}) async-start(), calls=%async_computation.3 | async-start | bytes 3932160 | tf_op jit(solution)/shard_map/all_gather | solution.py:89
  46.4 101.9 %reduce-scatter.2.cloned.1.call-start = ((), (), s32[]{:S(2)}) async-start(), calls=%async_computation.4 | async-start | bytes 3932160 | tf_op jit(solution)/shard_map/reduce_scatter | solution.py:93
  89.2 6.3 %copy-start.3 = (bf16[1,2048,1024]{2,1,0:T(8,128)(2,1)S(1)}, bf16[1,2048,1024]{2,1,0:T(8,128)(2,1)}, u32[]{:S(2)}) copy-start(bf16[1,2048,1024]{2,1,0:T(8,128)(2,1)} %param.19) | copy-start | bytes 12582916
  89.2 6.3 %copy-start.5 = (bf16[768,2048]{1,0:T(8,128)(2,1)S(1)}, bf16[768,2048]{1,0:T(8,128)(2,1)}, u32[]{:S(2)}) copy-start(bf16[768,2048]{1,0:T(8,128)(2,1)} %all-gather.2.cloned.1.call-done) | copy-start | bytes 9437188
  95.5 3.8 %copy-start.4 = (bf16[1,2048,1024]{2,1,0:T(8,128)(2,1)S(1)}, bf16[1,2048,1024]{2,1,0:T(8,128)(2,1)}, u32[]{:S(2)}) copy-start(bf16[1,2048,1024]{2,1,0:T(8,128)(2,1)} %param.21) | copy-start | bytes 12582916
  104.3 1.2 copy-start.1
  104.3 6.6 %copy-start.2 = (f32[192,2]{0,1:T(2,128)S(1)}, f32[192,2]{0,1:T(2,128)}, u32[]{:S(2)}) copy-start(f32[192,2]{0,1:T(2,128)} %param.18) | copy-start | bytes 4612
  109.3 43.8 %collective-permute-start = (bf16[15,512]{1,0:T(8,128)(2,1)S(1)}, bf16[15,512]{1,0:T(8,128)(2,1)S(1)}, u32[]{:S(2)}, u32[]{:S(2)}) collective-permute-start(bf16[15,512]{1,0:T(8,128)(2,1)S(1)} %slice.36), channel_id=1, source_target_pairs={{0,4},{4,8},{8,12},{12,16},{16,20},{20,24},{24,28},{1,5},{5,9},{9,... | collective-permute-start | bytes 46088 | tf_op jit(solution)/shard_map/ppermute | solution.py:14
  148.3 25.6 %all-to-all-start.1 = ((bf16[512,8,96]{0,2,1:T(8,128)(2,1)}), bf16[512,8,96]{0,2,1:T(8,128)(2,1)S(1)}, u32[]{:S(2)}, u32[]{:S(2)}) async-start(bf16[512,8,96]{0,2,1:T(8,128)(2,1)} %bitcast.71), calls=%async_computation.2 | async-start | bytes 1572864 | tf_op jit(solution)/shard_map/all_to_all | solution.py:102
  153.4 0.7 copy-start.6
Sparse Core Ops, SparseCore 0:
  46.5 42.6 all-gather.1
  104.4 43.8 reduce-scatter.1
where the time goes:
time: 185 us; the launch traced here: 184 us
  waiting for transfers between devices  98.8 us (53%)
  blocking collectives  27.2 us (15%)
  matrix products  16.7 us (9%)
  between operations  14.4 us (8%)
  local copies, waits for them, and re-layouts  12.8 us (7%)
  other arithmetic  8.08 us (4%)
  starting transfers between devices  6.26 us (3%)
    all_gather x1, waiting for transfers between devices, expert_half(): segment = lax.all_gather(arrived, 'tp', axis=1, tiled=True)  42.8 us
    reduce_scatter x1, waiting for transfers between devices, expert_half(): lax.psum_scatter(lax.dot_general(down_block, hidden, (((1,), (1,)), ((),...  37.4 us
    all_to_all x1, blocking collectives, expert_half(): lax.all_to_all(outgoing, 'ep', split_axis=0, concat_axis=0, tiled=True)  27.2 us
    all_to_all x1, waiting for transfers between devices, expert_half(): lax.all_to_all(results, 'ep', split_axis=1, concat_axis=1, tiled=True)  18.6 us
    dot_general x1, matrix products, expert_half(): up_part = jnp.dot(segment, up_block, preferred_element_type=jnp.float32)  6.28 us
    dot_general x1, matrix products, expert_half(): lax.dot_general(down_block, hidden, (((1,), (1,)), ((), ())), preferred_e...  4.88 us
    all_to_all x1, starting transfers between devices, expert_half(): lax.all_to_all(results, 'ep', split_axis=1, concat_axis=1, tiled=True)  4.61 us
    dot_general x1, matrix products, expert_half(): gate_part = jnp.dot(segment, gate_block, preferred_element_type=jnp.float32)  3.82 us
  transfers between devices with their start and end apart: 4, of which 3 were waited for; matrix products, arithmetic and copies ran while one was open for 3% of the time, Pallas kernels for 0%

commit v1 on v0

--- a/solution.py
+++ b/solution.py
@@ -86,7 +86,12 @@
     arrived = lax.all_to_all(outgoing, "ep", split_axis=0, concat_axis=0, tiled=True).reshape(
         experts * capacity, column_count
     )
-    segment = lax.all_gather(arrived, "tp", axis=1, tiled=True)
+    ring = [arrived]
+    for hop in range(3):
+        ring.append(lax.ppermute(ring[-1], "tp", [(dev, (dev + 1) % 4) for dev in range(4)]))
+    segment = jnp.roll(
+        jnp.concatenate(ring[::-1], axis=1), (lax.axis_index("tp") + 1) * ring[0].shape[1], axis=1
+    )
     gate_part = jnp.dot(segment, gate_block, preferred_element_type=jnp.float32)
     up_part = jnp.dot(segment, up_block, preferred_element_type=jnp.float32)
     hidden = (jax.nn.silu(gate_part) * up_part).astype(jnp.bfloat16)

time: 185 us -> 199 us (1.076)
  waiting for transfers between devices: 98.8 us -> 112 us
  matrix products: 16.7 us -> 13.8 us
  local copies, waits for them, and re-layouts: 12.8 us -> 15.1 us
    ppermute x0 -> x3, waiting for transfers between devices: none -> 54.9 us  [expert_half(): lax.ppermute(ring[-1], 'tp', [(dev, (dev + 1) % 4) for dev in range(4)])]
    all_gather x1 -> x0, waiting for transfers between devices: 42.8 us -> none  [expert_half(): segment = lax.all_gather(arrived, 'tp', axis=1, tiled=True)]
    dot_general x1, matrix products: 6.28 us -> 3.76 us  [expert_half(): up_part = jnp.dot(segment, up_block, preferred_element_type=jnp.float32)]
    unnamed x15 -> x22, local copies, waits for them, and re-layouts: 2.34 us -> 4.57 us
    ppermute x0 -> x3, starting transfers between devices: none -> 2.09 us  [expert_half(): lax.ppermute(ring[-1], 'tp', [(dev, (dev + 1) % 4) for dev in range(4)])]
  transfers between devices with their start and end apart: 4 -> 6, of which waited for: 3 -> 5; matrix products, arithmetic and copies ran while one was open for 3% -> 3% of each run, Pallas kernels for 0% -> 0%
where the time goes in v1:
time: 199 us
  waiting for transfers between devices  112 us (56%)
  blocking collectives  27.1 us (14%)
  local copies, waits for them, and re-layouts  15.1 us (8%)
  between operations  14.4 us (7%)
  matrix products  13.8 us (7%)
  other arithmetic  8.09 us (4%)
  starting transfers between devices  8.04 us (4%)
    ppermute x3, waiting for transfers between devices, expert_half(): lax.ppermute(ring[-1], 'tp', [(dev, (dev + 1) % 4) for dev in range(4)])  54.9 us
    reduce_scatter x1, waiting for transfers between devices, expert_half(): lax.psum_scatter(lax.dot_general(down_block, hidden, (((1,), (1,)), ((),...  38.6 us
    all_to_all x1, blocking collectives, expert_half(): lax.all_to_all(outgoing, 'ep', split_axis=0, concat_axis=0, tiled=True)  27.1 us
    all_to_all x1, waiting for transfers between devices, expert_half(): lax.all_to_all(results, 'ep', split_axis=1, concat_axis=1, tiled=True)  18.9 us
    dot_general x1, matrix products, expert_half(): lax.dot_general(down_block, hidden, (((1,), (1,)), ((), ())), preferred_e...  4.89 us
    all_to_all x1, starting transfers between devices, expert_half(): lax.all_to_all(results, 'ep', split_axis=1, concat_axis=1, tiled=True)  4.62 us
    unnamed x22, local copies, waits for them, and re-layouts  4.57 us
  transfers between devices with their start and end apart: 6, of which 5 were waited for; matrix products, arithmetic and copies ran while one was open for 3% of the time, Pallas kernels for 0%

profile of v1, /device:TPU:0, one launch (start us, length us, event | category | flops | bytes accessed | tf_op | source)
XLA Modules:
  0.0 199.0 jit_solution(13807569217259432192)
XLA Ops:
  7.2 0.0 copy-start
  7.2 0.0 reduce-scatter.2.cloned.1.call-start
  7.2 0.8 copy.14
  8.1 0.1 eq.32
  8.2 0.1 eq.28
  8.4 0.7 broadcast_multiply_fusion
  9.1 1.4 fusion.18
  10.4 0.9 reduce-window.6
  11.3 0.2 slice_reduce_fusion
  11.6 0.1 copy.13
  11.7 0.1 mul.102
  11.9 0.1 reshape.122
  12.0 0.1 fusion.33
  12.1 2.9 %scatter_custom_fusion = s32[768]{0:T(1024)S(1)} fusion(s32[384]{0:T(512)S(1)} %fusion.40, s32[384]{0:T(512)S(1)} %reshape.122, s32[]{:T(128)} %constant.86.clone.1), kind=kCustom, calls=%fused_computation.63 | custom fusion | bytes 3076 | tf_op jit(solution)/shard_map/scatter | solution.py:49
  15.1 1.4 fusion.20
  16.5 2.7 %gather_fusion = bf16[768,512]{1,0:T(8,128)(2,1)S(1)} fusion(bf16[193,512]{1,0:T(8,128)(2,1)S(1)} %pad_dynamic-slice_fusion.4, s32[1024]{0:T(1024)S(1)} %pad_clamp_fusion.1), kind=kCustom, calls=%fused_computation | custom fusion | bytes 1575936 | tf_op jit(solution)/shard_map/gather | solution.py:85
  19.2 27.1 %all_to_all.10 = bf16[8,96,512]{2,1,0:T(8,128)(2,1)S(1)} all-to-all(bf16[8,96,512]{2,1,0:T(8,128)(2,1)S(1)} %bitcast.68), channel_id=1, replica_groups=mesh['ep'=8,'tp'=4] {'ep'}, dimensions={0} | all-to-all | bytes 1572864 | tf_op jit(solution)/shard_map/all_to_all | solution.py:86
  46.3 1.5 collective-permute-start.1
  47.8 18.3 %collective-permute-done.1 = bf16[768,512]{1,0:T(8,128)(2,1)S(1)} collective-permute-done((bf16[768,512]{1,0:T(8,128)(2,1)S(1)}, bf16[768,512]{1,0:T(8,128)(2,1)S(1)}, u32[]{:S(2)}, u32[]{:S(2)}) %collective-permute-start.1) | collective-permute-done | bytes 786464 | tf_op jit(solution)/shard_map/ppermute | solution.py:91
  66.1 0.6 collective-permute-start.2
  66.7 18.4 %collective-permute-done.2 = bf16[768,512]{1,0:T(8,128)(2,1)S(1)} collective-permute-done((bf16[768,512]{1,0:T(8,128)(2,1)S(1)}, bf16[768,512]{1,0:T(8,128)(2,1)S(1)}, u32[]{:S(2)}, u32[]{:S(2)}) %collective-permute-start.2) | collective-permute-done | bytes 786464 | tf_op jit(solution)/shard_map/ppermute | solution.py:91
  85.0 0.0 collective-permute-start.3
  85.1 18.2 %collective-permute-done.3 = bf16[768,512]{1,0:T(8,128)(2,1)} collective-permute-done((bf16[768,512]{1,0:T(8,128)(2,1)S(1)}, bf16[768,512]{1,0:T(8,128)(2,1)}, u32[]{:S(2)}, u32[]{:S(2)}) %collective-permute-start.3) | collective-permute-done | bytes 786464 | tf_op jit(solution)/shard_map/ppermute | solution.py:91
  103.3 1.2 constant_dynamic-update-slice_fusion.7
  104.5 0.1 constant_dynamic-update-slice_fusion.6
  104.6 0.1 constant_dynamic-update-slice_fusion.5
  104.7 0.0 copy-start.3
  104.7 0.1 constant_dynamic-update-slice_fusion.4
  104.8 1.4 constant_dynamic-update-slice_fusion.3
  106.2 0.1 constant_dynamic-update-slice_fusion.2
  106.3 0.1 constant_dynamic-update-slice_fusion.1
  106.4 0.1 constant_dynamic-update-slice_fusion
  106.5 0.6 copy-done.3
  107.1 3.4 %fusion.4 = f32[768,1024]{1,0:T(8,128)S(1)} fusion(bf16[1,2048,1024]{2,1,0:T(8,128)(2,1)S(1)} %copy-done.3, bf16[768,4096]{1,0:T(8,128)(2,1)S(1)} %constant_dynamic-update-slice_fusion, s32[]{:T(128)S(6)} %select_n.48), kind=kOutput, calls=%fused_computation.7 | convolution fusion | flops 3221225472 | bytes 10485764 | tf_op jit(solution)/shard_map/dot_general | solution.py:95
  110.5 0.0 copy-done.4
  110.5 0.0 copy-start.5
  110.6 3.8 %multiply_convert_fusion = bf16[768,1024]{1,0:T(8,128)(2,1)S(1)} fusion(f32[768,1024]{1,0:T(8,128)S(1)} %fusion.4, bf16[1,2048,1024]{2,1,0:T(8,128)(2,1)S(1)} %copy-done.4, bf16[768,4096]{1,0:T(8,128)(2,1)S(1)} %constant_dynamic-update-slice_fusion, s32[]{:T(128)S(6)} %select_n.48), kind=kOutput, calls=%fused_computation.10 | convolution fusion | flops 3225944064 | bytes 12058628 | tf_op jit(solution)/shard_map/dot_general | solution.py:96
  114.3 0.0 copy-start.1
  114.4 4.9 %fusion.9 = bf16[2048,768]{0,1:T(8,128)(2,1)} fusion(bf16[768,1024]{1,0:T(8,128)(2,1)S(1)} %multiply_convert_fusion, bf16[1,2048,1024]{2,1,0:T(8,128)(2,1)S(1)} %copy-done.5), kind=kOutput, calls=%fused_computation.11 | convolution fusion | flops 3222798336 | bytes 8912896 | tf_op jit(solution)/shard_map/dot_general | solution.py:99
  119.2 0.0 reduce-scatter.2.cloned.1.call-update
  119.3 1.6 convert_element_type.53
  120.9 0.8 dynamic-slice
  121.7 0.3 multiply_reduce_fusion
  122.0 1.2 fusion.29
  123.1 1.3 collective-permute-start
  124.4 0.0 copy-done.2
  124.5 38.6 %reduce-scatter.2.cloned.1.call-done = bf16[512,768]{0,1:T(8,128)(2,1)} async-done(((bf16[2048,768]{0,1:T(8,128)(2,1)}), bf16[512,768]{0,1:T(8,128)(2,1)}) %reduce-scatter.2.cloned.1.call-update) | async-done | bytes 786448 | tf_op jit(solution)/shard_map/reduce_scatter | solution.py:98
  163.1 4.6 %all-to-all-start.1 = ((bf16[512,8,96]{0,2,1:T(8,128)(2,1)}), bf16[512,8,96]{0,2,1:T(8,128)(2,1)S(1)}, u32[]{:S(2)}, u32[]{:S(2)}) async-start(bf16[512,8,96]{0,2,1:T(8,128)(2,1)} %bitcast.71), calls=%async_computation.2 | async-start | bytes 1572864 | tf_op jit(solution)/shard_map/all_to_all | solution.py:107
  167.8 0.0 copy-start.6
  167.8 0.2 copy.16
  167.9 0.0 collective-permute-done
  168.0 0.1 maximum_convert_fusion
  168.0 0.1 pad_add_fusion.2
  168.2 0.1 pad_add_fusion.1
  168.3 0.1 pad_add_fusion
  168.4 0.1 add_bitcast_fusion
  168.5 0.0 copy-done
  168.5 0.0 copy-done.6
  168.6 1.2 fusion.21
  169.8 18.9 %all-to-all-done.1 = bf16[512,8,96]{0,2,1:T(8,128)(2,1)S(1)} async-done(((bf16[512,8,96]{0,2,1:T(8,128)(2,1)}), bf16[512,8,96]{0,2,1:T(8,128)(2,1)S(1)}, u32[]{:S(2)}, u32[]{:S(2)}) %all-to-all-start.1) | async-done | bytes 786464 | tf_op jit(solution)/shard_map/all_to_all | solution.py:107
  188.7 2.1 %gather_fusion.1 = bf16[384,512]{1,0:T(8,128)(2,1)S(1)} fusion(bf16[512,768]{0,1:T(8,128)(2,1)S(1)} %bitcast.59, s32[1024]{0:T(1024)S(1)} %pad_clamp_fusion), kind=kCustom, calls=%fused_computation.1 | custom fusion | bytes 787968 | tf_op jit(solution)/shard_map/gather | solution.py:111
  190.7 0.2 reshape.101
  190.9 0.6 fusion.42
  191.5 0.7 copy.19
  (19 shorter events, 0.2 us)
Async XLA Ops:
  7.2 161.4 %copy-start = (bf16[512,512]{1,0:T(8,128)(2,1)S(1)}, bf16[512,512]{1,0:T(8,128)(2,1)}, u32[]{:S(2)}) copy-start(bf16[512,512]{1,0:T(8,128)(2,1)} %param.13) | copy-start | bytes 1572868
  7.2 155.9 %reduce-scatter.2.cloned.1.call-start = ((), (), s32[]{:S(2)}) async-start(), calls=%async_computation.3 | async-start | bytes 3932160 | tf_op jit(solution)/shard_map/reduce_scatter | solution.py:98
  46.3 19.8 %collective-permute-start.1 = (bf16[768,512]{1,0:T(8,128)(2,1)S(1)}, bf16[768,512]{1,0:T(8,128)(2,1)S(1)}, u32[]{:S(2)}, u32[]{:S(2)}) collective-permute-start(bf16[768,512]{1,0:T(8,128)(2,1)S(1)} %bitcast.60), channel_id=1, source_target_pairs={{0,1},{1,2},{2,3},{3,0},{4,5},{5,6},{6,7},{7,4},{8,9},{9,10},{10,1... | collective-permute-start | bytes 2359304 | tf_op jit(solution)/shard_map/ppermute | solution.py:91
  66.1 19.0 %collective-permute-start.2 = (bf16[768,512]{1,0:T(8,128)(2,1)S(1)}, bf16[768,512]{1,0:T(8,128)(2,1)S(1)}, u32[]{:S(2)}, u32[]{:S(2)}) collective-permute-start(bf16[768,512]{1,0:T(8,128)(2,1)S(1)} %collective-permute-done.1), channel_id=1, source_target_pairs={{0,1},{1,2},{2,3},{3,0},{4,5},{5,6},{6,7},{7,4},{8,9},{9,10},{10,1... | collective-permute-start | bytes 2359304 | tf_op jit(solution)/shard_map/ppermute | solution.py:91
  85.0 18.2 %collective-permute-start.3 = (bf16[768,512]{1,0:T(8,128)(2,1)S(1)}, bf16[768,512]{1,0:T(8,128)(2,1)}, u32[]{:S(2)}, u32[]{:S(2)}) collective-permute-start(bf16[768,512]{1,0:T(8,128)(2,1)S(1)} %collective-permute-done.2), channel_id=1, source_target_pairs={{0,1},{1,2},{2,3},{3,0},{4,5},{5,6},{6,7},{7,4},{8,9},{9,10},{10,1... | collective-permute-start | bytes 2359304 | tf_op jit(solution)/shard_map/ppermute | solution.py:91
  104.7 2.4 %copy-start.3 = (bf16[1,2048,1024]{2,1,0:T(8,128)(2,1)S(1)}, bf16[1,2048,1024]{2,1,0:T(8,128)(2,1)}, u32[]{:S(2)}) copy-start(bf16[1,2048,1024]{2,1,0:T(8,128)(2,1)} %param.19) | copy-start | bytes 12582916
  107.1 3.4 %copy-start.4 = (bf16[1,2048,1024]{2,1,0:T(8,128)(2,1)S(1)}, bf16[1,2048,1024]{2,1,0:T(8,128)(2,1)}, u32[]{:S(2)}) copy-start(bf16[1,2048,1024]{2,1,0:T(8,128)(2,1)} %param.20) | copy-start | bytes 12582916
  110.5 3.8 %copy-start.5 = (bf16[1,2048,1024]{2,1,0:T(8,128)(2,1)S(1)}, bf16[1,2048,1024]{2,1,0:T(8,128)(2,1)}, u32[]{:S(2)}) copy-start(bf16[1,2048,1024]{2,1,0:T(8,128)(2,1)} %param.21) | copy-start | bytes 12582916
  114.3 4.9 %copy-start.1 = (bf16[256,2048]{1,0:T(8,128)(2,1)S(1)}, bf16[256,2048]{1,0:T(8,128)(2,1)}, u32[]{:S(2)}) copy-start(bf16[256,2048]{1,0:T(8,128)(2,1)} %param.11) | copy-start | bytes 3145732
  119.2 5.2 %copy-start.2 = (f32[192,2]{0,1:T(2,128)S(1)}, f32[192,2]{0,1:T(2,128)}, u32[]{:S(2)}) copy-start(f32[192,2]{0,1:T(2,128)} %param.18) | copy-start | bytes 4612
  123.1 44.8 %collective-permute-start = (bf16[15,512]{1,0:T(8,128)(2,1)S(1)}, bf16[15,512]{1,0:T(8,128)(2,1)S(1)}, u32[]{:S(2)}, u32[]{:S(2)}) collective-permute-start(bf16[15,512]{1,0:T(8,128)(2,1)S(1)} %slice.36), channel_id=1, source_target_pairs={{0,4},{4,8},{8,12},{12,16},{16,20},{20,24},{24,28},{1,5},{5,9},{9,... | collective-permute-start | bytes 46088 | tf_op jit(solution)/shard_map/ppermute | solution.py:14
  163.1 25.6 %all-to-all-start.1 = ((bf16[512,8,96]{0,2,1:T(8,128)(2,1)}), bf16[512,8,96]{0,2,1:T(8,128)(2,1)S(1)}, u32[]{:S(2)}, u32[]{:S(2)}) async-start(bf16[512,8,96]{0,2,1:T(8,128)(2,1)} %bitcast.71), calls=%async_computation.2 | async-start | bytes 1572864 | tf_op jit(solution)/shard_map/all_to_all | solution.py:107
  167.8 0.8 copy-start.6
Sparse Core Ops, SparseCore 0:
  119.4 43.6 reduce-scatter.1
